TPU v7x, 32 devices: a whole 2x2x4 slice. The times are simulated.
32 devices in a mesh: fs: 8 (over z, y), tp: 4 (over x, core).
Axes of the slice: x: 2, y: 2, z: 4, core: 2. Of those that a mesh axis runs over, the one named last changes fastest.
Arguments:
- inputs: bfloat16 [4096, 2112], P('fs', 'tp'), may hold values from -6 to 6
- w_conv_up: bfloat16 [2112, 2816], P('fs', 'tp'), may hold values from -0.125 to 0.125
- w_gate_up: bfloat16 [2112, 2816], P('fs', 'tp'), may hold values from -0.125 to 0.125
- w_down: bfloat16 [2816, 2112], P('tp', 'fs'), may hold values from -0.109375 to 0.109375
- taps: float32 [3, 2816], replicated, may hold values from -3 to 3
- conv_bias: float32 [2816], replicated, may hold values from -3 to 3
- cotangent: bfloat16 [4096, 2112], P('fs', 'tp'), may hold values from -6 to 6
Outputs:
- grad_inputs: bfloat16 [4096, 2112], P('fs', 'tp')
- grad_conv_up: float32 [2112, 2816], P('fs', 'tp')
- unit_norms: float32 [2816], P('tp')
- grad_taps: float32 [3, 2816], replicated
- grad_bias: float32 [2816], replicated
All inputs are finite; a program needn't handle non-finite values.
Results may differ from a plain program's by a relative error of at most 0.018.
Values may be sent and summed in bfloat16 or wider, within the bound.
A program may use at most 64 MiB of HBM per device.

v0:
```python
import math
import jax
import jax.numpy as jnp
from jax import lax
from jax.sharding import PartitionSpec as P

TAPS = 3


def shifted(block, axis, distance):
    devices = range(lax.axis_size(axis))
    route = [(i - distance, i) for i in devices if i - distance in devices]
    return lax.ppermute(block, axis, route)


def gelu_parts(value):
    normal_cdf = 0.5 * (1.0 + jax.scipy.special.erf(value / math.sqrt(2.0)))
    density = jnp.exp(-0.5 * value * value) / math.sqrt(2.0 * math.pi)
    return (value * normal_cdf, normal_cdf + value * density)


def per_device(inputs, w_conv_up, w_gate_up, w_down, taps, conv_bias, cotangent):
    span = TAPS - 1
    rows = inputs.shape[0]
    width = w_conv_up.shape[1]
    col_start = lax.axis_index("tp") * width
    taps_own = lax.dynamic_slice_in_dim(taps, col_start, width, 1)
    bias_own = lax.dynamic_slice_in_dim(conv_bias, col_start, width, 0)
    features, cot_full = (
        lax.all_gather(inputs, "tp", axis=1, tiled=True),
        lax.all_gather(cotangent, "tp", axis=1, tiled=True),
    )
    conv_weight, gate_weight = (
        lax.all_gather(w_conv_up, "fs", axis=0, tiled=True),
        lax.all_gather(w_gate_up, "fs", axis=0, tiled=True),
    )
    columns = cot_full
    d_hidden = lax.dot_general(
        columns,
        lax.all_gather(w_down, "fs", axis=1, tiled=True),
        (((1,), (1,)), ((), ())),
        preferred_element_type=jnp.float32,
    ).astype(jnp.bfloat16)
    up_a = jnp.dot(features, conv_weight, preferred_element_type=jnp.float32).astype(jnp.bfloat16)
    up_b = jnp.dot(features, gate_weight, preferred_element_type=jnp.float32).astype(jnp.bfloat16)
    earlier = shifted(up_a[rows - span :], "fs", 1)
    extended = jnp.concatenate([earlier, up_a], 0).astype(jnp.float32)
    conv_out = bias_own[None, :] + sum(
        (taps_own[i][None, :] * extended[i : i + rows] for i in range(TAPS))
    )
    gelu_value, gelu_slope = gelu_parts(conv_out)
    hidden_grad = d_hidden.astype(jnp.float32)
    d_conv = hidden_grad * up_b.astype(jnp.float32) * gelu_slope
    d_up_b = (hidden_grad * gelu_value).astype(jnp.bfloat16)
    later = shifted(d_conv[:span], "fs", -1)
    d_extended = jnp.concatenate([d_conv, later], 0)
    d_up_a = sum(
        (taps_own[i][None, :] * d_extended[span - i : span - i + rows] for i in range(TAPS))
    ).astype(jnp.bfloat16)
    tap_terms = [jnp.sum(d_conv * extended[i : i + rows], axis=0) for i in range(TAPS)]
    column_part = jnp.stack(tap_terms + [jnp.sum(d_conv, axis=0)], 0)
    contract = (((1,), (1,)), ((), ()))
    partial_sum = lax.dot_general(d_up_a, conv_weight, contract, preferred_element_type=jnp.float32)
    partial_sum = partial_sum + lax.dot_general(
        d_up_b, gate_weight, contract, preferred_element_type=jnp.float32
    )
    grad_inputs = lax.psum_scatter(
        partial_sum.astype(jnp.bfloat16), "tp", scatter_dimension=1, tiled=True
    )
    columns = features
    grad_conv_up = lax.psum_scatter(
        lax.dot_general(
            columns, d_up_a, (((0,), (0,)), ((), ())), preferred_element_type=jnp.float32
        ),
        "fs",
        scatter_dimension=0,
        tiled=True,
    )
    squares = jnp.sum(grad_conv_up * grad_conv_up, axis=0)
    placed = jnp.zeros((TAPS + 1, width * lax.axis_size("tp")), jnp.float32)
    placed = lax.dynamic_update_slice_in_dim(placed, column_part, col_start, 1)
    full_columns = lax.psum(placed, ("fs", "tp"))
    unit_norms = lax.psum(squares, "fs")
    return (grad_inputs, grad_conv_up, unit_norms, full_columns[:TAPS], full_columns[TAPS])


def solution(mesh):
    return jax.shard_map(
        per_device,
        mesh=mesh,
        in_specs=(
            P("fs", "tp"),
            P("fs", "tp"),
            P("fs", "tp"),
            P("tp", "fs"),
            P(),
            P(),
            P("fs", "tp"),
        ),
        out_specs=(P("fs", "tp"), P("fs", "tp"), P("tp"), P(), P()),
        check_vma=False,
    )
```

profile of v0, /device:TPU:0, one launch (start us, length us, event | category | flops | bytes accessed | tf_op | source)
XLA Modules:
  0.0 441.5 jit_solution(5598248172429005860)
XLA Ops:
  7.2 0.0 all-gather.10.cloned.1.call-start
  7.2 0.7 all-gather.10.cloned.1.call-update
  7.9 0.0 all-gather.14.cloned.1.call-start
  7.9 0.7 all-gather.14.cloned.1.call-update
  8.6 0.0 all-gather.6.cloned.1.call-start
  8.7 0.7 all-gather.6.cloned.1.call-update
  9.4 0.0 all-gather.8.cloned.1.call-start
  9.4 0.5 all-gather.8.cloned.1.call-update
  10.0 0.0 all-gather.12.cloned.1.call-start
  10.0 0.5 all-gather.12.cloned.1.call-update
  10.5 0.0 reduce-scatter.7.cloned.1.call-start
  10.6 0.8 dynamic_slice.7
  11.4 0.9 dynamic-slice_reduce_fusion.2
  12.3 22.9 %all-gather.10.cloned.1.call-done = bf16[512,2112]{0,1:T(8,128)(2,1)} async-done(((bf16[512,528]{0,1:T(8,128)(2,1)}), bf16[512,2112]{0,1:T(8,128)(2,1)}) %all-gather.10.cloned.1.call-update) | async-done | bytes 2162704 | tf_op jit(solution)/shard_map/all_gather | solution.py:30
  35.2 63.3 %all-gather.14.cloned.1.call-done = bf16[2112,704]{1,0:T(8,128)(2,1)} async-done(((bf16[264,704]{1,0:T(8,128)(2,1)}), bf16[2112,704]{1,0:T(8,128)(2,1)}) %all-gather.14.cloned.1.call-update) | async-done | bytes 2973712 | tf_op jit(solution)/shard_map/all_gather | solution.py:34
  98.5 4.5 %convolution_convert_fusion = bf16[512,704]{0,1:T(8,128)(2,1)S(1)} fusion(bf16[512,2112]{0,1:T(8,128)(2,1)} %all-gather.10.cloned.1.call-done, bf16[2112,704]{1,0:T(8,128)(2,1)} %all-gather.14.cloned.1.call-done), kind=kOutput, calls=%fused_computation.26 | convolution fusion | flops 1522892800 | bytes 5857280 | tf_op jit(solution)/shard_map/dot_general | solution.py:44
  102.9 0.1 slice.54
  103.1 2.5 collective-permute-start
  105.5 16.1 %all-gather.6.cloned.1.call-done = bf16[512,2112]{0,1:T(8,128)(2,1)} async-done(((bf16[512,528]{0,1:T(8,128)(2,1)}), bf16[512,2112]{0,1:T(8,128)(2,1)}) %all-gather.6.cloned.1.call-update) | async-done | bytes 2162704 | tf_op jit(solution)/shard_map/all_gather | solution.py:31
  121.7 63.1 %all-gather.8.cloned.1.call-done = bf16[704,2112]{0,1:T(8,128)(2,1)} async-done(((bf16[704,264]{0,1:T(8,128)(2,1)}), bf16[704,2112]{0,1:T(8,128)(2,1)}) %all-gather.8.cloned.1.call-update) | async-done | bytes 2973712 | tf_op jit(solution)/shard_map/all_gather | solution.py:40
  184.8 4.5 %convolution_convert_fusion.2 = bf16[512,704]{0,1:T(8,128)(2,1)S(1)} fusion(bf16[512,2112]{0,1:T(8,128)(2,1)} %all-gather.6.cloned.1.call-done, bf16[704,2112]{0,1:T(8,128)(2,1)} %all-gather.8.cloned.1.call-done), kind=kOutput, calls=%fused_computation.28 | convolution fusion | flops 1522892800 | bytes 5857280 | tf_op jit(solution)/shard_map/dot_general | solution.py:38
  189.3 0.0 collective-permute-done
  189.3 0.4 maximum_convert_fusion
  189.7 2.4 add_add_fusion
  192.1 54.5 %all-gather.12.cloned.1.call-done = bf16[2112,704]{1,0:T(8,128)(2,1)} async-done(((bf16[264,704]{1,0:T(8,128)(2,1)}), bf16[2112,704]{1,0:T(8,128)(2,1)}) %all-gather.12.cloned.1.call-update) | async-done | bytes 2973712 | tf_op jit(solution)/shard_map/all_gather | solution.py:35
  246.6 5.3 %fusion.6 = f32[512,704]{0,1:T(8,128)S(1)} fusion(bf16[512,704]{0,1:T(8,128)(2,1)S(1)} %convolution_convert_fusion.2, f32[512,704]{0,1:T(8,128)} %add_add_fusion, bf16[512,2112]{0,1:T(8,128)(2,1)} %all-gather.10.cloned.1.call-done, bf16[2112,704]{1,0:T(8,128)(2,1)} %all-gather.12.cloned.1.call-done), kind=kOutput, calls=%fused_computation.13 | convolution fusion | flops 1527218176 | bytes 8740864 | tf_op jit(solution)/shard_map/dot_general | solution.py:45
  251.9 0.0 copy-start
  251.9 1.4 collective-permute-start.1
  253.4 9.0 %collective-permute-done.1 = f32[2,704]{0,1:T(8,128)S(1)} collective-permute-done((f32[2,704]{0,1:T(8,128)S(1)}, f32[2,704]{0,1:T(8,128)S(1)}, u32[]{:S(2)}, u32[]{:S(2)}) %collective-permute-start.1) | collective-permute-done | bytes 5664 | tf_op jit(solution)/shard_map/ppermute | solution.py:13
  262.3 3.2 multiply_reduce_fusion.2
  265.6 0.0 copy-done
  265.6 4.5 %convolution_bitcast_fusion = f32[2112,704]{0,1:T(8,128)} fusion(bf16[512,704]{0,1:T(8,128)(2,1)S(1)} %get-tuple-element.22, bf16[512,2112]{0,1:T(8,128)(2,1)S(1)} %copy-done), kind=kOutput, calls=%fused_computation | convolution fusion | flops 1522532352 | bytes 8830976 | tf_op jit(solution)/shard_map/dot_general | solution.py:72
  270.1 7.2 %copy.14 = f32[2112,704]{1,0:T(8,128)} copy(f32[2112,704]{0,1:T(8,128)} %convolution_bitcast_fusion) | data formatting | bytes 11894784
  277.3 0.0 reduce-scatter.7.cloned.1.call-update
  277.3 0.0 copy-start.1
  277.3 0.2 reduce-scatter.5.cloned.1.call-start
  277.5 3.9 fusion.14
  281.5 3.3 fusion
  284.8 0.0 reduce-scatter.5.cloned.1.call-update
  284.9 0.3 dynamic_update_slice.3
  285.2 44.6 %psum.15 = f32[4,2816]{1,0:T(4,128)S(1)} all-reduce(f32[4,2816]{1,0:T(4,128)S(1)} %dynamic_update_slice.3), channel_id=1, replica_groups=mesh['fs'=8,'tp'=4] {'fs','tp'}, use_global_device_ids=true, to_apply=%region_8.0 | all-reduce | flops 11264 | bytes 90112 | tf_op jit(solution)/shard_map/psum | solution.py:82
  329.9 0.0 copy-start.2
  329.9 0.6 slice_reduce_fusion
  330.5 70.1 %reduce-scatter.7.cloned.1.call-done = f32[264,704]{1,0:T(8,128)} async-done(((f32[2112,704]{1,0:T(8,128)}), f32[264,704]{1,0:T(8,128)}) %reduce-scatter.7.cloned.1.call-update) | async-done | bytes 743440
  400.6 1.5 copy.15
  402.1 0.2 multiply_reduce_fusion.3
  402.3 20.3 %psum.14 = f32[704]{0:T(1024)} all-reduce(f32[704]{0:T(1024)S(1)} %multiply_reduce_fusion.3), channel_id=1, replica_groups=mesh['fs'=8,'tp'=4] {'fs'}, use_global_device_ids=true, to_apply=%region_3.0 | all-reduce | flops 704 | bytes 5632 | tf_op jit(solution)/shard_map/psum | solution.py:83
  422.6 12.0 %reduce-scatter.5.cloned.1.call-done = bf16[512,528]{0,1:T(8,128)(2,1)} async-done(((bf16[512,2112]{0,1:T(8,128)(2,1)}), bf16[512,528]{0,1:T(8,128)(2,1)}) %reduce-scatter.5.cloned.1.call-update) | async-done | bytes 540688 | tf_op jit(solution)/shard_map/reduce_scatter | solution.py:67
  (11 shorter events, 0.1 us)
Async XLA Ops:
  7.2 28.1 %all-gather.10.cloned.1.call-start = ((), (), s32[]{:S(2)}) async-start(), calls=%async_computation.4 | async-start | bytes 2703360 | tf_op jit(solution)/shard_map/all_gather | solution.py:30
  7.9 90.6 %all-gather.14.cloned.1.call-start = ((), (), s32[]{:S(2)}) async-start(), calls=%async_computation.6 | async-start | bytes 3649536 | tf_op jit(solution)/shard_map/all_gather | solution.py:34
  8.6 113.0 %all-gather.6.cloned.1.call-start = ((), (), s32[]{:S(2)}) async-start(), calls=%async_computation.2 | async-start | bytes 2703360 | tf_op jit(solution)/shard_map/all_gather | solution.py:31
  9.4 175.4 %all-gather.8.cloned.1.call-start = ((), (), s32[]{:S(2)}) async-start(), calls=%async_computation.3 | async-start | bytes 3649536 | tf_op jit(solution)/shard_map/all_gather | solution.py:40
  10.0 236.7 %all-gather.12.cloned.1.call-start = ((), (), s32[]{:S(2)}) async-start(), calls=%async_computation.5 | async-start | bytes 3649536 | tf_op jit(solution)/shard_map/all_gather | solution.py:35
  10.5 390.1 %reduce-scatter.7.cloned.1.call-start = ((), (), s32[]{:S(2)}) async-start(), calls=%async_computation.8 | async-start | bytes 7299072
  103.1 86.2 %collective-permute-start = (bf16[2,704]{0,1:T(8,128)(2,1)S(1)}, bf16[2,704]{0,1:T(8,128)(2,1)S(1)}, u32[]{:S(2)}, u32[]{:S(2)}) collective-permute-start(bf16[2,704]{0,1:T(8,128)(2,1)S(1)} %slice.54), channel_id=1, source_target_pairs={{0,4},{4,8},{8,12},{12,16},{16,20},{20,24},{24,28},{1,5},{5,9},{9,... | collective-permute-start | bytes 8456 | tf_op jit(solution)/shard_map/ppermute | solution.py:13
  251.9 13.6 %copy-start = (bf16[512,2112]{0,1:T(8,128)(2,1)S(1)}, bf16[512,2112]{0,1:T(8,128)(2,1)}, u32[]{:S(2)}) copy-start(bf16[512,2112]{0,1:T(8,128)(2,1)} %all-gather.10.cloned.1.call-done) | copy-start | bytes 6488068
  251.9 10.4 %collective-permute-start.1 = (f32[2,704]{0,1:T(8,128)S(1)}, f32[2,704]{0,1:T(8,128)S(1)}, u32[]{:S(2)}, u32[]{:S(2)}) collective-permute-start(f32[2,704]{0,1:T(8,128)S(1)} %slice.58), channel_id=1, source_target_pairs={{4,0},{8,4},{12,8},{16,12},{20,16},{24,20},{28,24},{5,1},{9,5},{13... | collective-permute-start | bytes 16904 | tf_op jit(solution)/shard_map/ppermute | solution.py:13
  277.3 4.2 copy-start.1
  277.3 157.3 %reduce-scatter.5.cloned.1.call-start = ((), (), s32[]{:S(2)}) async-start(), calls=%async_computation.7 | async-start | bytes 2703360 | tf_op jit(solution)/shard_map/reduce_scatter | solution.py:67
  277.5 3.9 copy-start.3
  329.9 72.4 %copy-start.2 = (f32[4,2816]{1,0:T(4,128)}, f32[4,2816]{1,0:T(4,128)S(1)}, u32[]{:S(2)}) copy-start(f32[4,2816]{1,0:T(4,128)S(1)} %psum.15) | copy-start | bytes 135172
Sparse Core Ops, SparseCore 0:
  9.5 25.6 all-gather.9
  37.4 61.0 all-gather.13
  100.1 21.5 all-gather.5
  123.7 61.0 all-gather.7
  186.8 59.7 all-gather.11
  277.4 123.1 reduce-scatter.6
  403.7 30.8 reduce-scatter.4
where the time goes:
time: 442 us; the launch traced here: 441 us
  waiting for transfers between devices  314 us (71%)
  blocking collectives  64.9 us (15%)
  matrix products  25.9 us (6%)
  between operations  14.3 us (3%)
  local copies, waits for them, and re-layouts  11.5 us (3%)
  other arithmetic  6.2 us (1%)
    unnamed x8, waiting for transfers between devices  73.2 us
    all_gather x1, waiting for transfers between devices, per_device(): lax.all_gather(w_conv_up, 'fs', axis=0, tiled=True)  63.3 us
    all_gather x1, waiting for transfers between devices, per_device(): lax.all_gather(w_down, 'fs', axis=1, tiled=True)  63.1 us
    all_gather x1, waiting for transfers between devices, per_device(): lax.all_gather(w_gate_up, 'fs', axis=0, tiled=True)  54.5 us
    psum x1, blocking collectives, per_device(): full_columns = lax.psum(placed, ('fs', 'tp'))  44.6 us
    all_gather x1, waiting for transfers between devices, per_device(): lax.all_gather(inputs, 'tp', axis=1, tiled=True)  22.9 us
    psum x1, blocking collectives, per_device(): unit_norms = lax.psum(squares, 'fs')  20.3 us
    all_gather x1, waiting for transfers between devices, per_device(): lax.all_gather(cotangent, 'tp', axis=1, tiled=True)  16.1 us
  transfers between devices with their start and end apart: 9, of which 8 were waited for; matrix products, arithmetic and copies ran while one was open for 5% of the time, Pallas kernels for 0%

commit v1 on v0

--- a/solution.py
+++ b/solution.py
@@ -79,7 +79,7 @@
     squares = jnp.sum(grad_conv_up * grad_conv_up, axis=0)
     placed = jnp.zeros((TAPS + 1, width * lax.axis_size("tp")), jnp.float32)
     placed = lax.dynamic_update_slice_in_dim(placed, column_part, col_start, 1)
-    full_columns = lax.psum(placed, ("fs", "tp"))
+    full_columns = jnp.sum(lax.all_gather(placed, ("fs", "tp")), axis=0)
     unit_norms = lax.psum(squares, "fs")
     return (grad_inputs, grad_conv_up, unit_norms, full_columns[:TAPS], full_columns[TAPS])
 

time: 442 us -> 488 us (1.10)
  waiting for transfers between devices: 314 us -> 401 us
  blocking collectives: 64.9 us -> 20.2 us
    unnamed x8 -> x9, waiting for transfers between devices: 73.2 us -> 126 us
    psum x1 -> x0, blocking collectives: 44.6 us -> none  [per_device(): full_columns = lax.psum(placed, ('fs', 'tp'))]
    all_gather x0 -> x1, waiting for transfers between devices: none -> 34.3 us  [per_device(): full_columns = jnp.sum(lax.all_gather(placed, ('fs', 'tp')), axis=0)]
  transfers between devices with their start and end apart: 9 -> 10, of which waited for: 8 -> 9; matrix products, arithmetic and copies ran while one was open for 5% -> 8% of each run, Pallas kernels for 0% -> 0%
where the time goes in v1:
time: 488 us; the launch traced here: 487 us
  waiting for transfers between devices  401 us (82%)
  matrix products  27.5 us (6%)
  blocking collectives  20.2 us (4%)
  between operations  14.3 us (3%)
  local copies, waits for them, and re-layouts  12.1 us (2%)
  other arithmetic  7.78 us (2%)
    unnamed x9, waiting for transfers between devices  126 us
    all_gather x1, waiting for transfers between devices, per_device(): lax.all_gather(w_conv_up, 'fs', axis=0, tiled=True)  63.3 us
    all_gather x1, waiting for transfers between devices, per_device(): lax.all_gather(w_down, 'fs', axis=1, tiled=True)  63.1 us
    all_gather x1, waiting for transfers between devices, per_device(): lax.all_gather(w_gate_up, 'fs', axis=0, tiled=True)  54.5 us
    all_gather x1, waiting for transfers between devices, per_device(): full_columns = jnp.sum(lax.all_gather(placed, ('fs', 'tp')), axis=0)  34.3 us
    all_gather x1, waiting for transfers between devices, per_device(): lax.all_gather(inputs, 'tp', axis=1, tiled=True)  22.9 us
    psum x1, blocking collectives, per_device(): unit_norms = lax.psum(squares, 'fs')  20.2 us
    all_gather x1, waiting for transfers between devices, per_device(): lax.all_gather(cotangent, 'tp', axis=1, tiled=True)  16.1 us
  transfers between devices with their start and end apart: 10, of which 9 were waited for; matrix products, arithmetic and copies ran while one was open for 8% of the time, Pallas kernels for 0%

profile of v1, /device:TPU:0, one launch (start us, length us, event | category | flops | bytes accessed | tf_op | source)
XLA Modules:
  0.0 487.4 jit_solution(14230752323974878052)
XLA Ops:
  7.2 0.0 all-gather.11.cloned.1.call-start
  7.2 0.7 all-gather.11.cloned.1.call-update
  7.9 0.0 all-gather.15.cloned.1.call-start
  7.9 0.7 all-gather.15.cloned.1.call-update
  8.6 0.0 all-gather.7.cloned.1.call-start
  8.7 0.7 all-gather.7.cloned.1.call-update
  9.4 0.0 all-gather.9.cloned.1.call-start
  9.4 0.5 all-gather.9.cloned.1.call-update
  10.0 0.0 all-gather.13.cloned.1.call-start
  10.0 0.5 all-gather.13.cloned.1.call-update
  10.5 0.0 all-gather.17.cloned.1.call-start
  10.6 0.8 dynamic_slice.7
  11.4 0.9 dynamic-slice_reduce_fusion.2
  12.3 22.9 %all-gather.11.cloned.1.call-done = bf16[512,2112]{0,1:T(8,128)(2,1)} async-done(((bf16[512,528]{0,1:T(8,128)(2,1)}), bf16[512,2112]{0,1:T(8,128)(2,1)}) %all-gather.11.cloned.1.call-update) | async-done | bytes 2162704 | tf_op jit(solution)/shard_map/all_gather | solution.py:30
  35.2 63.3 %all-gather.15.cloned.1.call-done = bf16[2112,704]{1,0:T(8,128)(2,1)} async-done(((bf16[264,704]{1,0:T(8,128)(2,1)}), bf16[2112,704]{1,0:T(8,128)(2,1)}) %all-gather.15.cloned.1.call-update) | async-done | bytes 2973712 | tf_op jit(solution)/shard_map/all_gather | solution.py:34
  98.5 4.5 convolution_convert_fusion
  102.9 0.1 slice.54
  103.1 2.5 collective-permute-start
  105.5 16.1 %all-gather.7.cloned.1.call-done = bf16[512,2112]{0,1:T(8,128)(2,1)} async-done(((bf16[512,528]{0,1:T(8,128)(2,1)}), bf16[512,2112]{0,1:T(8,128)(2,1)}) %all-gather.7.cloned.1.call-update) | async-done | bytes 2162704 | tf_op jit(solution)/shard_map/all_gather | solution.py:31
  121.7 63.1 %all-gather.9.cloned.1.call-done = bf16[704,2112]{0,1:T(8,128)(2,1)} async-done(((bf16[704,264]{0,1:T(8,128)(2,1)}), bf16[704,2112]{0,1:T(8,128)(2,1)}) %all-gather.9.cloned.1.call-update) | async-done | bytes 2973712 | tf_op jit(solution)/shard_map/all_gather | solution.py:40
  184.8 4.5 convolution_convert_fusion.2
  189.3 0.4 maximum_convert_fusion
  189.7 2.4 add_add_fusion
  192.1 54.5 %all-gather.13.cloned.1.call-done = bf16[2112,704]{1,0:T(8,128)(2,1)} async-done(((bf16[264,704]{1,0:T(8,128)(2,1)}), bf16[2112,704]{1,0:T(8,128)(2,1)}) %all-gather.13.cloned.1.call-update) | async-done | bytes 2973712 | tf_op jit(solution)/shard_map/all_gather | solution.py:35
  246.6 5.3 %fusion.6 = f32[512,704]{0,1:T(8,128)S(1)} fusion(bf16[512,704]{0,1:T(8,128)(2,1)S(1)} %convolution_convert_fusion.2, f32[512,704]{0,1:T(8,128)} %add_add_fusion, bf16[512,2112]{0,1:T(8,128)(2,1)} %all-gather.11.cloned.1.call-done, bf16[2112,704]{1,0:T(8,128)(2,1)} %all-gather.13.cloned.1.call-done), kind=kOutput, calls=%fused_computation.13 | convolution fusion | flops 1527218176 | bytes 8740864 | tf_op jit(solution)/shard_map/dot_general | solution.py:45
  251.9 1.3 collective-permute-start.1
  253.2 9.0 %collective-permute-done.1 = f32[2,704]{0,1:T(8,128)S(1)} collective-permute-done((f32[2,704]{0,1:T(8,128)S(1)}, f32[2,704]{0,1:T(8,128)S(1)}, u32[]{:S(2)}, u32[]{:S(2)}) %collective-permute-start.1) | collective-permute-done | bytes 5664 | tf_op jit(solution)/shard_map/ppermute | solution.py:13
  262.2 3.2 multiply_reduce_fusion.2
  265.5 0.3 dynamic_update_slice.4
  265.8 0.0 copy-start.1
  265.8 0.6 copy-done.1
  266.5 0.0 all-gather.17.cloned.1.call-update
  266.5 0.0 reduce-scatter.7.cloned.1.call-start
  266.5 6.1 %convolution_bitcast_fusion = f32[2112,704]{0,1:T(8,128)} fusion(bf16[512,704]{0,1:T(8,128)(2,1)S(1)} %get-tuple-element.22, bf16[512,2112]{0,1:T(8,128)(2,1)} %all-gather.11.cloned.1.call-done), kind=kOutput, calls=%fused_computation | convolution fusion | flops 1522532352 | bytes 8830976 | tf_op jit(solution)/shard_map/dot_general | solution.py:72
  272.6 7.2 %copy.14 = f32[2112,704]{1,0:T(8,128)} copy(f32[2112,704]{0,1:T(8,128)} %convolution_bitcast_fusion) | data formatting | bytes 11894784
  279.8 0.0 reduce-scatter.7.cloned.1.call-update
  279.9 0.2 reduce-scatter.5.cloned.1.call-start
  280.1 3.9 fusion.14
  284.0 3.3 fusion
  287.4 0.0 reduce-scatter.5.cloned.1.call-update
  287.4 34.3 %all-gather.17.cloned.1.call-done = f32[32,4,2816]{2,1,0:T(4,128)} async-done(((f32[1,4,2816]{2,1,0:T(4,128)}), f32[32,4,2816]{2,1,0:T(4,128)}) %all-gather.17.cloned.1.call-update) | async-done | bytes 1441808 | tf_op jit(solution)/shard_map/all_gather | solution.py:82
  321.7 1.6 reduce_sum.59
  323.2 0.6 slice_reduce_fusion
  323.9 122.7 %reduce-scatter.7.cloned.1.call-done = f32[264,704]{1,0:T(8,128)} async-done(((f32[2112,704]{1,0:T(8,128)}), f32[264,704]{1,0:T(8,128)}) %reduce-scatter.7.cloned.1.call-update) | async-done | bytes 743440
  446.6 1.5 copy.15
  448.1 0.2 multiply_reduce_fusion.3
  448.3 20.2 %psum.7 = f32[704]{0:T(1024)} all-reduce(f32[704]{0:T(1024)S(1)} %multiply_reduce_fusion.3), channel_id=1, replica_groups=mesh['fs'=8,'tp'=4] {'fs'}, use_global_device_ids=true, to_apply=%region_3.0 | all-reduce | flops 704 | bytes 5632 | tf_op jit(solution)/shard_map/psum | solution.py:83
  468.6 12.0 %reduce-scatter.5.cloned.1.call-done = bf16[512,528]{0,1:T(8,128)(2,1)} async-done(((bf16[512,2112]{0,1:T(8,128)(2,1)}), bf16[512,528]{0,1:T(8,128)(2,1)}) %reduce-scatter.5.cloned.1.call-update) | async-done | bytes 540688 | tf_op jit(solution)/shard_map/reduce_scatter | solution.py:67
  (14 shorter events, 0.1 us)
Async XLA Ops:
  7.2 28.1 %all-gather.11.cloned.1.call-start = ((), (), s32[]{:S(2)}) async-start(), calls=%async_computation.4 | async-start | bytes 2703360 | tf_op jit(solution)/shard_map/all_gather | solution.py:30
  7.9 90.6 %all-gather.15.cloned.1.call-start = ((), (), s32[]{:S(2)}) async-start(), calls=%async_computation.6 | async-start | bytes 3649536 | tf_op jit(solution)/shard_map/all_gather | solution.py:34
  8.6 113.0 %all-gather.7.cloned.1.call-start = ((), (), s32[]{:S(2)}) async-start(), calls=%async_computation.2 | async-start | bytes 2703360 | tf_op jit(solution)/shard_map/all_gather | solution.py:31
  9.4 175.4 %all-gather.9.cloned.1.call-start = ((), (), s32[]{:S(2)}) async-start(), calls=%async_computation.3 | async-start | bytes 3649536 | tf_op jit(solution)/shard_map/all_gather | solution.py:40
  10.0 236.7 %all-gather.13.cloned.1.call-start = ((), (), s32[]{:S(2)}) async-start(), calls=%async_computation.5 | async-start | bytes 3649536 | tf_op jit(solution)/shard_map/all_gather | solution.py:35
  10.5 311.1 %all-gather.17.cloned.1.call-start = ((), (), s32[]{:S(2)}) async-start(), calls=%async_computation.8 | async-start | bytes 1486848 | tf_op jit(solution)/shard_map/all_gather | solution.py:82
  103.1 86.2 %collective-permute-start = (bf16[2,704]{0,1:T(8,128)(2,1)S(1)}, bf16[2,704]{0,1:T(8,128)(2,1)S(1)}, u32[]{:S(2)}, u32[]{:S(2)}) collective-permute-start(bf16[2,704]{0,1:T(8,128)(2,1)S(1)} %slice.54), channel_id=1, source_target_pairs={{0,4},{4,8},{8,12},{12,16},{16,20},{20,24},{24,28},{1,5},{5,9},{9,... | collective-permute-start | bytes 8456 | tf_op jit(solution)/shard_map/ppermute | solution.py:13
  251.9 10.3 %collective-permute-start.1 = (f32[2,704]{0,1:T(8,128)S(1)}, f32[2,704]{0,1:T(8,128)S(1)}, u32[]{:S(2)}, u32[]{:S(2)}) collective-permute-start(f32[2,704]{0,1:T(8,128)S(1)} %slice.58), channel_id=1, source_target_pairs={{4,0},{8,4},{12,8},{16,12},{20,16},{24,20},{28,24},{5,1},{9,5},{13... | collective-permute-start | bytes 16904 | tf_op jit(solution)/shard_map/ppermute | solution.py:13
  265.8 0.6 copy-start.1
  266.5 180.1 %reduce-scatter.7.cloned.1.call-start = ((), (), s32[]{:S(2)}) async-start(), calls=%async_computation.9 | async-start | bytes 7299072
  279.9 4.2 copy-start
  279.9 200.7 %reduce-scatter.5.cloned.1.call-start = ((), (), s32[]{:S(2)}) async-start(), calls=%async_computation.7 | async-start | bytes 2703360 | tf_op jit(solution)/shard_map/reduce_scatter | solution.py:67
  280.1 3.9 copy-start.3
  323.2 125.1 %copy-start.2 = (f32[4,2816]{1,0:T(4,128)}, f32[4,2816]{1,0:T(4,128)S(1)}, u32[]{:S(2)}) copy-start(f32[4,2816]{1,0:T(4,128)S(1)} %reduce_sum.59) | copy-start | bytes 135172
Sparse Core Ops, SparseCore 0:
  9.5 25.6 all-gather.10
  37.4 61.0 all-gather.14
  100.1 21.5 all-gather.6
  123.7 61.0 all-gather.8
  186.8 59.7 all-gather.12
  266.6 55.0 all-gather.16
  325.8 120.7 reduce-scatter.6
  449.7 30.7 reduce-scatter.4
